TPU v7x, 32 devices: a whole 2x2x4 slice. The times are simulated.
32 devices in a mesh: grp: 2 (over y), sp: 4 (over z), tp: 4 (over x, core).
Axes of the slice: x: 2, y: 2, z: 4, core: 2. Of those that a mesh axis runs over, the one named last changes fastest.
Arguments:
- tokens: bfloat16 [1280, 2048], P(('grp', 'sp')), parts along dimension 0, may hold values from -6 to 6
- norm_gain: float32 [2048], replicated, may hold values from 0.6 to 5
- query_weight: bfloat16 [2048, 2048], P('sp', 'tp')
- key_weight: bfloat16 [2048, 512], P('sp', 'tp')
- value_weight: bfloat16 [2048, 512], P('sp', 'tp'), may hold values from -0.125 to 0.125
- map_lambda: float32 [16], P('tp'), may hold values from 0.3 to 0.8
- head_gain: float32 [16, 128], P('tp'), may hold values from 0.1 to 1.9
- attn_out_weight: bfloat16 [2048, 2048], P('tp', 'sp'), may hold values from -0.125 to 0.125
- pool_out_weight: bfloat16 [2048, 2048], P('tp', 'sp'), may hold values from -0.09375 to 0.09375
Outputs:
- mixed_rows: bfloat16 [1280, 2048], P(('grp', 'sp', 'tp')), parts along dimension 0
- log_totals: float32 [2, 16, 1280], P(None, 'tp', ('grp', 'sp')), parts along dimension 2
There are 2 independent parts, one for each index of `grp`. A program takes and returns all parts, laid end to end along the dimension named above; an argument that names none is the same for every part. Nothing has to cross between parts.
All inputs are finite; a program needn't handle non-finite values.
Results may differ from a plain program's by a relative error of at most 0.013.
The roundings to bfloat16 on the way count: a program that leaves them out, or rounds other values in their place, can miss the bound.
Values may be sent and summed in bfloat16 or wider, within the bound.
A program may use at most 64 MiB of HBM per device.

v0:
```python
import math
import jax
import jax.numpy as jnp
from jax import lax
from jax.sharding import PartitionSpec as P

HD = 64
VD = 128
POOL_SPAN = 16
epsilon = 1e-06
very_low = -1e30


def extended(cells, sides, width):
    for axis, dim in sides:
        count = lax.axis_size(axis)
        ends = count - 1
        head = lax.slice_in_dim(cells, 0, width, axis=dim)
        tail = lax.slice_in_dim(cells, cells.shape[dim] - width, cells.shape[dim], axis=dim)
        cells = jnp.concatenate(
            [
                lax.ppermute(tail, axis, [(i, (i + 1) % count) for i in range(ends)]),
                cells,
                lax.ppermute(head, axis, [((i + 1) % count, i) for i in range(ends)]),
            ],
            axis=dim,
        )
    return cells


def add_products(totals, pieces, source):
    results = []
    for running, piece in zip(totals, pieces):
        results.append(jnp.dot(source, piece, preferred_element_type=jnp.float32))
    return tuple(results)


def on_device(
    tokens,
    norm_gain,
    query_weight,
    key_weight,
    value_weight,
    map_lambda,
    head_gain,
    attn_out_weight,
    pool_out_weight,
):
    tokens_wide = tokens.astype(jnp.float32)
    normed = (
        tokens_wide
        * lax.rsqrt(jnp.mean(tokens_wide * tokens_wide, axis=-1, keepdims=True) + epsilon)
        * norm_gain
    ).astype(jnp.bfloat16)
    row_count = normed.shape[0]
    sp_index = lax.axis_index("sp")
    tp_index = lax.axis_index("tp")
    group_width = pool_out_weight.shape[0]
    local_heads = map_lambda.shape[0]
    key_heads = value_weight.shape[1] // VD
    group_heads = local_heads // key_heads
    q_empty = jnp.zeros((row_count, query_weight.shape[1]), jnp.float32)
    k_empty = jnp.zeros((row_count, key_weight.shape[1]), jnp.float32)
    v_empty = jnp.zeros((row_count, value_weight.shape[1]), jnp.float32)
    q_acc, k_acc, v_acc = add_products(
        (q_empty, k_empty, v_empty),
        (
            lax.all_gather(query_weight, "sp", axis=0, tiled=True),
            lax.all_gather(key_weight, "sp", axis=0, tiled=True),
            lax.all_gather(value_weight, "sp", axis=0, tiled=True),
        ),
        normed,
    )
    queries = q_acc.astype(jnp.bfloat16).reshape(row_count, key_heads, group_heads, 2, HD)
    keys_flat = k_acc.astype(jnp.bfloat16)
    values_flat = v_acc.astype(jnp.bfloat16)

    def key_block(state_now, key_pair):
        maxima, totals, accums = state_now
        key_blk, val_blk = key_pair
        scores = jnp.einsum(
            "qhgmd,khmd->hgmqk", queries, key_blk, preferred_element_type=jnp.float32
        ) * HD ** (-0.5)
        highest = jnp.maximum(maxima, jnp.max(scores, axis=-1))
        factor = jnp.exp(maxima - highest)
        weights = jnp.exp(scores - highest[..., None])
        totals = totals * factor + jnp.sum(weights, axis=-1)
        accums = accums * factor[..., None] + jnp.einsum(
            "hgmqk,khe->hgmqe",
            weights.astype(jnp.bfloat16),
            val_blk,
            preferred_element_type=jnp.float32,
        )
        return ((highest, totals, accums), None)

    start_state = (
        jnp.full((key_heads, group_heads, 2, row_count), very_low, jnp.float32),
        jnp.zeros((key_heads, group_heads, 2, row_count), jnp.float32),
        jnp.zeros((key_heads, group_heads, 2, row_count, VD), jnp.float32),
    )
    key_piece = lax.all_gather(keys_flat, "sp", axis=0, tiled=True)
    val_piece = lax.all_gather(values_flat, "sp", axis=0, tiled=True)
    piece_len = key_piece.shape[0]
    block_len = math.gcd(piece_len, 512)
    key_blocks = key_piece.reshape(piece_len // block_len, block_len, key_heads, 2, HD)
    val_blocks = val_piece.reshape(piece_len // block_len, block_len, key_heads, VD)
    state_next, unused = lax.scan(key_block, start_state, (key_blocks, val_blocks))
    maxima, totals, accums = state_next
    log_parts = maxima + jnp.log(totals)
    log_totals = jnp.transpose(log_parts, (2, 0, 1, 3)).reshape(2, local_heads, row_count)
    reads = accums / totals[..., None]
    contrast = reads[:, :, 0] - map_lambda.reshape(key_heads, group_heads, 1, 1) * reads[:, :, 1]
    scaled = (
        contrast
        * lax.rsqrt(jnp.mean(contrast * contrast, axis=-1, keepdims=True) + epsilon)
        * head_gain.reshape(key_heads, group_heads, 1, VD)
    )
    attention_head_rows = (
        jnp.transpose(scaled, (2, 0, 1, 3))
        .reshape(row_count, local_heads * VD)
        .astype(jnp.bfloat16)
    )
    head_rows, log_totals = (attention_head_rows, log_totals)
    own_chan = lax.dynamic_slice_in_dim(normed, tp_index * group_width, group_width, 1)
    reach = POOL_SPAN // 2
    padded = extended(own_chan, (("sp", 0),), reach)
    window = jnp.left_shift(jnp.int32(2), tp_index)
    half_span = window // 2
    running = jnp.zeros((row_count, group_width), jnp.float32)
    for offset in range(POOL_SPAN):
        piece = lax.dynamic_slice_in_dim(padded, reach - half_span + offset, row_count, 0).astype(
            jnp.float32
        )
        running = running + jnp.where(offset < window, piece, 0.0)
    seq_len = row_count * lax.axis_size("sp")
    position = sp_index * row_count + jnp.arange(row_count, dtype=jnp.int32)
    lower_edge = jnp.clip(position - half_span, 0, seq_len)
    upper_edge = jnp.clip(position + window - half_span, 0, seq_len)
    counts_f = (upper_edge - lower_edge).astype(jnp.float32)[:, None]
    pooled = (running / counts_f - own_chan.astype(jnp.float32)).astype(jnp.bfloat16)
    attn_whole, pool_whole = (
        lax.all_gather(attn_out_weight, "sp", axis=1, tiled=True),
        lax.all_gather(pool_out_weight, "sp", axis=1, tiled=True),
    )
    mixed = lax.psum_scatter(
        (
            jnp.dot(head_rows, attn_whole, preferred_element_type=jnp.float32)
            + jnp.dot(pooled, pool_whole, preferred_element_type=jnp.float32)
        ).astype(jnp.bfloat16),
        "tp",
        scatter_dimension=0,
        tiled=True,
    )
    return (mixed, log_totals)


def solution(mesh):
    placed = (
        P(("grp", "sp"), None),
        P(),
        P("sp", "tp"),
        P("sp", "tp"),
        P("sp", "tp"),
        P("tp"),
        P("tp", None),
        P("tp", "sp"),
        P("tp", "sp"),
    )
    return jax.shard_map(
        on_device,
        mesh=mesh,
        in_specs=placed,
        out_specs=(P(("grp", "sp", "tp"), None), P(None, "tp", ("grp", "sp"))),
        check_vma=False,
    )
```

profile of v0, /device:TPU:0, one launch (start us, length us, event | category | flops | bytes accessed | tf_op | source)
XLA Modules:
  0.0 200.9 jit_solution(6198464641306412881)
XLA Ops:
  7.2 0.0 all-gather.4.cloned.1.call-start
  7.2 0.7 all-gather.4.cloned.1.call-update
  7.9 0.0 all-gather.6.cloned.1.call-start
  8.0 0.7 all-gather.6.cloned.1.call-update
  8.7 0.0 all-gather.8.cloned.1.call-start
  8.7 1.3 fusion.15
  10.0 1.0 fusion.17
  11.0 5.0 %collective-permute-start = (bf16[8,512]{1,0:T(8,128)(2,1)S(1)}, bf16[8,512]{1,0:T(8,128)(2,1)S(1)}, u32[]{:S(2)}, u32[]{:S(2)}) collective-permute-start(bf16[8,512]{1,0:T(8,128)(2,1)S(1)} %get-tuple-element.102), channel_id=1, source_target_pairs={{0,4},{4,8},{8,12},{1,5},{5,9},{9,13},{2,6},{6,10},{10,14},{3,7},{... | collective-permute-start | bytes 24584 | tf_op jit(solution)/shard_map/ppermute | solution.py:22
  16.0 1.3 collective-permute-start.1
  17.3 0.0 all-gather.8.cloned.1.call-update
  17.3 0.0 reduce-scatter.2.cloned.1.call-start
  17.4 24.1 %all_gather.21 = bf16[2048,128]{1,0:T(8,128)(2,1)S(1)} all-gather(bf16[512,128]{1,0:T(8,128)(2,1)S(1)} %copy-done.1), channel_id=1, replica_groups=mesh['grp'=2,'sp'=4,'tp'=4] {'sp'}, dimensions={0}, use_global_device_ids=true | all-gather | bytes 655360 | tf_op jit(solution)/shard_map/all_gather | solution.py:69
  41.5 0.3 convolution_convert_fusion.2
  41.9 15.2 %all_gather.22 = bf16[640,128]{1,0:T(8,128)(2,1)S(1)} all-gather(bf16[160,128]{1,0:T(8,128)(2,1)S(1)} %convolution_convert_fusion.2), channel_id=1, replica_groups=mesh['grp'=2,'sp'=4,'tp'=4] {'sp'}, dimensions={0}, use_global_device_ids=true | all-gather | bytes 204800 | tf_op jit(solution)/shard_map/all_gather | solution.py:101
  57.1 21.5 %all_gather.24 = bf16[2048,128]{1,0:T(8,128)(2,1)S(1)} all-gather(bf16[512,128]{1,0:T(8,128)(2,1)S(1)} %copy-done.2), channel_id=1, replica_groups=mesh['grp'=2,'sp'=4,'tp'=4] {'sp'}, dimensions={0}, use_global_device_ids=true | all-gather | bytes 655360 | tf_op jit(solution)/shard_map/all_gather | solution.py:70
  78.5 0.3 convolution_convert_fusion.1
  78.9 14.8 %all_gather.25 = bf16[640,128]{1,0:T(8,128)(2,1)S(1)} all-gather(bf16[160,128]{1,0:T(8,128)(2,1)S(1)} %convolution_convert_fusion.1), channel_id=1, replica_groups=mesh['grp'=2,'sp'=4,'tp'=4] {'sp'}, dimensions={0}, use_global_device_ids=true | all-gather | bytes 204800 | tf_op jit(solution)/shard_map/all_gather | solution.py:102
  93.7 0.2 reshape.142
  93.8 0.2 copy.22
  94.2 0.0 all-gather.4.cloned.1.call-done
  94.2 2.1 %convolution_convert_fusion = bf16[160,512]{1,0:T(8,128)(2,1)S(1)} fusion(bf16[160,2048]{1,0:T(8,128)(2,1)S(1)} %fusion.17, bf16[2048,512]{1,0:T(8,128)(2,1)} %all-gather.4.cloned.1.call-done), kind=kOutput, calls=%fused_computation.29 | convolution fusion | flops 335626240 | bytes 2916352 | tf_op jit(solution)/shard_map/dot_general | solution.py:34
  96.4 0.1 copy.21
  96.6 8.5 %while.15 = (s32[]{:T(128)}, f32[1,4,2,160]{3,1,2,0:T(4,128)S(1)}, f32[1,4,2,160]{3,1,2,0:T(4,128)S(1)}, f32[1,4,2,160,128]{4,3,2,1,0:T(8,128)S(1)}, bf16[5,128,...) while((s32[]{:T(128)}, f32[1,4,2,160]{3,1,2,0:T(4,128)S(1)}, ...), condition=%wide.region_4.5_spmd.clone, body=%wide.region_1.4_spmd.clone.sunk | while | flops 64232960 | bytes 3694705 | solution.py:107
  96.6 0.6 fusion.78
  97.2 0.6 fusion.80
  97.8 0.4 fusion.81
  98.3 0.6 fusion.78
  98.9 0.6 fusion.80
  99.5 0.4 fusion.81
  100.0 0.6 fusion.78
  100.6 0.6 fusion.80
  101.2 0.4 fusion.81
  101.7 0.6 fusion.78
  102.3 0.6 fusion.80
  102.9 0.4 fusion.81
  103.4 0.6 fusion.78
  104.0 0.6 fusion.80
  104.6 0.4 fusion.81
  105.1 0.2 broadcast_divide_fusion
  105.3 0.3 multiply_reduce_fusion
  105.6 0.2 fusion.20
  105.8 0.1 copy.27
  105.9 16.4 %all-gather.6.cloned.1.call-done = bf16[512,2048]{1,0:T(8,128)(2,1)} async-done(((bf16[512,512]{1,0:T(8,128)(2,1)}), bf16[512,2048]{1,0:T(8,128)(2,1)}) %all-gather.6.cloned.1.call-update) | async-done | bytes 2097168 | tf_op jit(solution)/shard_map/all_gather | solution.py:142
  122.4 2.1 %fusion.21 = f32[160,2048]{1,0:T(8,128)S(1)} fusion(bf16[512,2048]{1,0:T(8,128)(2,1)} %all-gather.6.cloned.1.call-done, bf16[20,8,4,128]{3,2,1,0:T(4,128)(2,1)S(1)} %bitcast.102), kind=kOutput, calls=%fused_computation.42 | convolution fusion | flops 335544320 | bytes 3571712 | tf_op jit(solution)/shard_map/dot_general | solution.py:147
  124.5 44.1 %all-gather.8.cloned.1.call-done = bf16[512,2048]{1,0:T(8,128)(2,1)} async-done(((bf16[512,512]{1,0:T(8,128)(2,1)}), bf16[512,2048]{1,0:T(8,128)(2,1)}) %all-gather.8.cloned.1.call-update) | async-done | bytes 2097168 | tf_op jit(solution)/shard_map/all_gather | solution.py:143
  168.6 4.3 %fusion.14 = bf16[160,2048]{1,0:T(8,128)(2,1)} fusion(f32[160,2048]{1,0:T(8,128)S(1)} %fusion.21, bf16[512,2048]{1,0:T(8,128)(2,1)} %all-gather.8.cloned.1.call-done, bf16[160,512]{1,0:T(8,128)(2,1)S(1)} %constant_dynamic-slice_fusion.1, f32[160]{0:T(256)S(1)} %subtract_convert_fusion.2, bf16[176,512]{1,0:T(8,128)(2,1)S(1)} %pad_maximum_fusion, ...), kind=kOutput, calls=%fused_computation.23 | convolution fusion | flops 340377600 | bytes 6849616 | tf_op jit(solution)/shard_map/dot_general | solution.py:148
  172.9 0.6 add_bitcast_fusion
  173.5 20.8 %reduce-scatter.2.cloned.1.call-done = bf16[40,2048]{1,0:T(8,128)(2,1)} async-done(((bf16[160,2048]{1,0:T(8,128)(2,1)}), bf16[40,2048]{1,0:T(8,128)(2,1)}) %reduce-scatter.2.cloned.1.call-update) | async-done | bytes 163856 | tf_op jit(solution)/shard_map/reduce_scatter | solution.py:145
  (44 shorter events, 0.4 us)
Async XLA Ops:
  7.2 2.9 %copy-start = (bf16[160,2048]{1,0:T(8,128)(2,1)S(1)}, bf16[160,2048]{1,0:T(8,128)(2,1)}, u32[]{:S(2)}) copy-start(bf16[160,2048]{1,0:T(8,128)(2,1)} %param.11) | copy-start | bytes 1966084
  7.2 10.3 %copy-start.1 = (bf16[512,128]{1,0:T(8,128)(2,1)S(1)}, bf16[512,128]{1,0:T(8,128)(2,1)}, u32[]{:S(2)}) copy-start(bf16[512,128]{1,0:T(8,128)(2,1)} %param.14) | copy-start | bytes 393220
  7.2 87.0 %all-gather.4.cloned.1.call-start = ((), (), s32[]{:S(2)}) async-start(), calls=%async_computation.1 | async-start | bytes 2621440 | tf_op jit(solution)/shard_map/all_gather | solution.py:68
  7.9 114.4 %all-gather.6.cloned.1.call-start = ((), (), s32[]{:S(2)}) async-start(), calls=%async_computation.2 | async-start | bytes 2621440 | tf_op jit(solution)/shard_map/all_gather | solution.py:142
  8.7 159.9 %all-gather.8.cloned.1.call-start = ((), (), s32[]{:S(2)}) async-start(), calls=%async_computation.3 | async-start | bytes 2621440 | tf_op jit(solution)/shard_map/all_gather | solution.py:143
  10.0 47.0 %copy-start.2 = (bf16[512,128]{1,0:T(8,128)(2,1)S(1)}, bf16[512,128]{1,0:T(8,128)(2,1)}, u32[]{:S(2)}) copy-start(bf16[512,128]{1,0:T(8,128)(2,1)} %param.15) | copy-start | bytes 393220
  11.0 83.1 %collective-permute-start = (bf16[8,512]{1,0:T(8,128)(2,1)S(1)}, bf16[8,512]{1,0:T(8,128)(2,1)S(1)}, u32[]{:S(2)}, u32[]{:S(2)}) collective-permute-start(bf16[8,512]{1,0:T(8,128)(2,1)S(1)} %get-tuple-element.102), channel_id=1, source_target_pairs={{0,4},{4,8},{8,12},{1,5},{5,9},{9,13},{2,6},{6,10},{10,14},{3,7},{... | collective-permute-start | bytes 24584 | tf_op jit(solution)/shard_map/ppermute | solution.py:22
  16.0 78.2 %collective-permute-start.1 = (bf16[8,512]{1,0:T(8,128)(2,1)S(1)}, bf16[8,512]{1,0:T(8,128)(2,1)S(1)}, u32[]{:S(2)}, u32[]{:S(2)}) collective-permute-start(bf16[8,512]{1,0:T(8,128)(2,1)S(1)} %get-tuple-element.103), channel_id=1, source_target_pairs={{4,0},{8,4},{12,8},{5,1},{9,5},{13,9},{6,2},{10,6},{14,10},{7,3},{... | collective-permute-start | bytes 24584 | tf_op jit(solution)/shard_map/ppermute | solution.py:24
  17.3 177.0 %reduce-scatter.2.cloned.1.call-start = ((), (), s32[]{:S(2)}) async-start(), calls=%async_computation.4 | async-start | bytes 819200 | tf_op jit(solution)/shard_map/reduce_scatter | solution.py:145
  96.5 8.8 %copy-start.4 = (f32[4]{0:T(128)S(1)}, f32[4]{0:T(128)}, u32[]{:S(2)}) copy-start(f32[4]{0:T(128)} %param.16) | copy-start | bytes 52
  96.5 9.1 %copy-start.3 = (f32[4,128]{1,0:T(4,128)S(1)}, f32[4,128]{1,0:T(4,128)}, u32[]{:S(2)}) copy-start(f32[4,128]{1,0:T(4,128)} %param.17) | copy-start | bytes 6148
Sparse Core Ops, SparseCore 0:
  9.6 66.0 all-gather.3
  77.3 45.0 all-gather.5
  123.9 44.6 all-gather.7
  173.1 21.2 reduce-scatter.1
where the time goes:
time: 201 us
  waiting for transfers between devices  82.8 us (41%)
  blocking collectives  75.5 us (38%)
  matrix products  14.4 us (7%)
  between operations  14.2 us (7%)
  other arithmetic  6.68 us (3%)
  starting transfers between devices  6.4 us (3%)
    all_gather x1, waiting for transfers between devices, on_device(): lax.all_gather(pool_out_weight, 'sp', axis=1, tiled=True)  44.1 us
    all_gather x1, blocking collectives, on_device(): lax.all_gather(key_weight, 'sp', axis=0, tiled=True)  24.1 us
    all_gather x1, blocking collectives, on_device(): lax.all_gather(value_weight, 'sp', axis=0, tiled=True)  21.5 us
    reduce_scatter x1, waiting for transfers between devices, on_device(): lax.psum_scatter((jnp.dot(head_rows, attn_whole, preferred_element_type=j...  20.8 us
    all_gather x1, waiting for transfers between devices, on_device(): lax.all_gather(attn_out_weight, 'sp', axis=1, tiled=True)  16.4 us
    all_gather x1, blocking collectives, on_device(): key_piece = lax.all_gather(keys_flat, 'sp', axis=0, tiled=True)  15.2 us
    all_gather x1, blocking collectives, on_device(): val_piece = lax.all_gather(values_flat, 'sp', axis=0, tiled=True)  14.8 us
    ppermute x1, starting transfers between devices, extended(): lax.ppermute(tail, axis, [(i, (i + 1) % count) for i in range(ends)])  4.96 us
  transfers between devices with their start and end apart: 6, of which 3 were waited for; matrix products, arithmetic and copies ran while one was open for 9% of the time, Pallas kernels for 0%

commit v1 on v0

--- a/solution.py
+++ b/solution.py
@@ -9,6 +9,19 @@
 POOL_SPAN = 16
 epsilon = 1e-06
 very_low = -1e30
+
+
+def gather_around(x, axis, dim):
+    ways = lax.axis_size(axis)
+    up = [(d, (d + 1) % ways) for d in range(ways)]
+    down = [(d, (d - 1) % ways) for d in range(ways)]
+    earlier, later = ([x], [x])
+    for _ in range(ways // 2):
+        earlier.append(lax.ppermute(earlier[-1], axis, up))
+    for _ in range((ways - 1) // 2):
+        later.append(lax.ppermute(later[-1], axis, down))
+    line = jnp.concatenate([*earlier[::-1], *later[1:]], axis=dim)
+    return jnp.roll(line, (lax.axis_index(axis) - ways // 2) * x.shape[dim], axis=dim)
 
 
 def extended(cells, sides, width):
@@ -140,7 +153,7 @@
     pooled = (running / counts_f - own_chan.astype(jnp.float32)).astype(jnp.bfloat16)
     attn_whole, pool_whole = (
         lax.all_gather(attn_out_weight, "sp", axis=1, tiled=True),
-        lax.all_gather(pool_out_weight, "sp", axis=1, tiled=True),
+        gather_around(pool_out_weight, "sp", 1),
     )
     mixed = lax.psum_scatter(
         (

time: 201 us -> 226 us (1.12)
  blocking collectives: 75.5 us -> 136 us
  waiting for transfers between devices: 82.8 us -> 24.2 us
  local copies, waits for them, and re-layouts: 0.68 us -> 11.7 us
  matrix products: 14.4 us -> 21.7 us
  starting transfers between devices: 6.4 us -> 9.04 us
    all_gather x1 -> x0, waiting for transfers between devices: 44.1 us -> none  [on_device(): lax.all_gather(pool_out_weight, 'sp', axis=1, tiled=True)]
    all_gather x1, blocking collectives: 24.1 us -> 58 us  [on_device(): lax.all_gather(key_weight, 'sp', axis=0, tiled=True)]
    all_gather x1, blocking collectives: 15.2 us -> 45.6 us  [on_device(): key_piece = lax.all_gather(keys_flat, 'sp', axis=0, tiled=True)]
    all_gather x1, waiting for transfers between devices: 16.4 us -> 0.02 us  [on_device(): lax.all_gather(attn_out_weight, 'sp', axis=1, tiled=True)]
    unnamed x12 -> x21, local copies, waits for them, and re-layouts: 0.23 us -> 8.13 us
    ppermute x0 -> x3, starting transfers between devices: none -> 5.8 us  [the longest x2 3.7 us: gather_around(): earlier.append(lax.ppermute(earlier[-1], axis, up))]
    dot_general x5, matrix products: 3.18 us -> 6.96 us  [key_block(): jnp.einsum('qhgmd,khmd->hgmqk', queries, key_blk, preferred_element_type=...]
    dot_general x5, matrix products: 1.94 us -> 5.61 us  [key_block(): jnp.einsum('hgmqk,khe->hgmqe', weights.astype(jnp.bfloat16), val_blk, pre...]
  transfers between devices with their start and end apart: 6 -> 8, of which waited for: 3 -> 1; matrix products, arithmetic and copies ran while one was open for 9% -> 16% of each run, Pallas kernels for 0% -> 0%
where the time goes in v1:
time: 226 us; the launch traced here: 225 us
  blocking collectives  136 us (60%)
  waiting for transfers between devices  24.2 us (11%)
  matrix products  21.7 us (10%)
  between operations  14 us (6%)
  local copies, waits for them, and re-layouts  11.7 us (5%)
  starting transfers between devices  9.04 us (4%)
  other arithmetic  8.66 us (4%)
    all_gather x1, blocking collectives, on_device(): lax.all_gather(key_weight, 'sp', axis=0, tiled=True)  58 us
    all_gather x1, blocking collectives, on_device(): key_piece = lax.all_gather(keys_flat, 'sp', axis=0, tiled=True)  45.6 us
    reduce_scatter x1, waiting for transfers between devices, on_device(): lax.psum_scatter((jnp.dot(head_rows, attn_whole, preferred_element_type=j...  23.4 us
    all_gather x1, blocking collectives, on_device(): lax.all_gather(value_weight, 'sp', axis=0, tiled=True)  18 us
    all_gather x1, blocking collectives, on_device(): val_piece = lax.all_gather(values_flat, 'sp', axis=0, tiled=True)  14.2 us
    unnamed x21, local copies, waits for them, and re-layouts  8.13 us
    dot_general x5, matrix products, key_block(): jnp.einsum('qhgmd,khmd->hgmqk', queries, key_blk, preferred_element_type=...  6.96 us
    dot_general x5, matrix products, key_block(): jnp.einsum('hgmqk,khe->hgmqe', weights.astype(jnp.bfloat16), val_blk, pre...  5.61 us
  transfers between devices with their start and end apart: 8, of which 1 were waited for; matrix products, arithmetic and copies ran while one was open for 16% of the time, Pallas kernels for 0%

profile of v1, /device:TPU:0, one launch (start us, length us, event | category | flops | bytes accessed | tf_op | source)
XLA Modules:
  0.0 225.3 jit_solution(9163375397561729329)
XLA Ops:
  7.2 0.7 all-gather.3.cloned.1.call-update
  8.0 3.1 %collective-permute-start.2 = (bf16[512,512]{1,0:T(8,128)(2,1)}, bf16[512,512]{1,0:T(8,128)(2,1)S(1)}, u32[]{:S(2)}, u32[]{:S(2)}) collective-permute-start(bf16[512,512]{1,0:T(8,128)(2,1)} %param.19), channel_id=1, source_target_pairs={{0,4},{4,8},{8,12},{12,0},{1,5},{5,9},{9,13},{13,1},{2,6},{6,10},{... | collective-permute-start | bytes 1572872 | tf_op jit(solution)/shard_map/ppermute | solution.py:20
  11.1 2.1 collective-permute-start.4
  13.2 1.3 fusion.16
  14.5 1.3 fusion.18
  15.8 1.8 collective-permute-start
  17.6 1.3 collective-permute-start.1
  19.1 58.0 %all_gather.18 = bf16[2048,128]{1,0:T(8,128)(2,1)S(1)} all-gather(bf16[512,128]{1,0:T(8,128)(2,1)} %param.14), channel_id=1, replica_groups=mesh['grp'=2,'sp'=4,'tp'=4] {'sp'}, dimensions={0}, use_global_device_ids=true | all-gather | bytes 655360 | tf_op jit(solution)/shard_map/all_gather | solution.py:82
  77.1 0.7 constant_dynamic-slice_fusion.1
  77.7 18.0 %all_gather.21 = bf16[2048,128]{1,0:T(8,128)(2,1)S(1)} all-gather(bf16[512,128]{1,0:T(8,128)(2,1)S(1)} %copy-done.3), channel_id=1, replica_groups=mesh['grp'=2,'sp'=4,'tp'=4] {'sp'}, dimensions={0}, use_global_device_ids=true | all-gather | bytes 655360 | tf_op jit(solution)/shard_map/all_gather | solution.py:83
  95.7 0.3 convolution_convert_fusion.2
  96.0 0.6 collective-permute-start.3
  96.7 45.6 %all_gather.19 = bf16[640,128]{1,0:T(8,128)(2,1)} all-gather(bf16[160,128]{1,0:T(8,128)(2,1)S(1)} %convolution_convert_fusion.2), channel_id=1, replica_groups=mesh['grp'=2,'sp'=4,'tp'=4] {'sp'}, dimensions={0}, use_global_device_ids=true | all-gather | bytes 204800 | tf_op jit(solution)/shard_map/all_gather | solution.py:114
  142.2 0.3 convolution_convert_fusion.1
  142.6 14.2 %all_gather.22 = bf16[640,128]{1,0:T(8,128)(2,1)} all-gather(bf16[160,128]{1,0:T(8,128)(2,1)S(1)} %convolution_convert_fusion.1), channel_id=1, replica_groups=mesh['grp'=2,'sp'=4,'tp'=4] {'sp'}, dimensions={0}, use_global_device_ids=true | all-gather | bytes 204800 | tf_op jit(solution)/shard_map/all_gather | solution.py:115
  156.7 1.8 reshape.142
  158.6 1.8 copy.22
  160.4 1.6 pad_maximum_fusion
  162.0 0.9 constant_dynamic-update-slice_fusion.7
  162.9 0.9 constant_dynamic-update-slice_fusion.6
  163.7 0.9 constant_dynamic-update-slice_fusion.5
  164.6 0.9 constant_dynamic-update-slice_fusion.4
  165.5 0.9 constant_dynamic-update-slice_fusion.3
  166.4 0.9 constant_dynamic-update-slice_fusion.2
  167.4 0.9 constant_dynamic-update-slice_fusion.1
  168.3 0.9 constant_dynamic-update-slice_fusion
  169.1 2.1 convolution_convert_fusion
  171.4 16.0 %while.15 = (s32[]{:T(128)}, f32[1,4,2,160]{3,1,2,0:T(4,128)S(1)}, f32[1,4,2,160]{3,1,2,0:T(4,128)S(1)}, f32[1,4,2,160,128]{4,3,2,1,0:T(8,128)S(1)}, bf16[5,128,...) while((s32[]{:T(128)}, f32[1,4,2,160]{3,1,2,0:T(4,128)S(1)}, ...), condition=%wide.region_4.5_spmd.clone, body=%wide.region_1.4_spmd.clone.sunk | while | flops 64232960 | bytes 3593337 | solution.py:120
  171.5 1.4 fusion.78
  172.9 0.6 fusion.80
  173.5 1.1 fusion.81
  174.6 1.4 fusion.78
  176.1 0.6 fusion.80
  176.7 1.1 fusion.81
  177.8 1.4 fusion.78
  179.3 0.6 fusion.80
  179.9 1.1 fusion.81
  181.0 1.4 fusion.78
  182.5 0.6 fusion.80
  183.1 1.1 fusion.81
  184.2 1.4 fusion.78
  185.7 0.6 fusion.80
  186.3 1.1 fusion.81
  187.7 0.3 multiply_reduce_fusion
  188.3 2.1 fusion.22
  190.4 4.3 %fusion.14 = bf16[160,2048]{1,0:T(8,128)(2,1)} fusion(f32[160,2048]{1,0:T(8,128)S(1)} %fusion.22, bf16[512,4096]{1,0:T(8,128)(2,1)} %constant_dynamic-update-slice_fusion, s32[]{:T(128)S(6)} %select_n.217, bf16[160,512]{1,0:T(8,128)(2,1)S(1)} %copy-done.1, f32[160]{0:T(256)S(1)} %subtract_convert_fusion.2, bf16[176,512]{1,0:T(8,128)(2,1)S(1)} %copy-done.2, ...), kind=kOutput, calls=%fused_computation.23 | convolution fusion | flops 340377600 | bytes 6849620 | tf_op jit(solution)/shard_map/dot_general | solution.py:161
  194.7 0.6 add_bitcast_fusion
  195.4 23.4 %reduce-scatter.2.cloned.1.call-done = bf16[40,2048]{1,0:T(8,128)(2,1)} async-done(((bf16[160,2048]{1,0:T(8,128)(2,1)}), bf16[40,2048]{1,0:T(8,128)(2,1)}) %reduce-scatter.2.cloned.1.call-update) | async-done | bytes 163856 | tf_op jit(solution)/shard_map/reduce_scatter | solution.py:158
  (57 shorter events, 1.1 us)
Async XLA Ops:
  7.2 70.6 %copy-start.3 = (bf16[512,128]{1,0:T(8,128)(2,1)S(1)}, bf16[512,128]{1,0:T(8,128)(2,1)}, u32[]{:S(2)}) copy-start(bf16[512,128]{1,0:T(8,128)(2,1)} %param.15) | copy-start | bytes 393220
  7.2 162.0 %all-gather.3.cloned.1.call-start = ((), (), s32[]{:S(2)}) async-start(), calls=%async_computation.1 | async-start | bytes 2621440 | tf_op jit(solution)/shard_map/all_gather | solution.py:81
  7.9 180.4 %all-gather.5.cloned.1.call-start = ((), (), s32[]{:S(2)}) async-start(), calls=%async_computation.2 | async-start | bytes 2621440 | tf_op jit(solution)/shard_map/all_gather | solution.py:155
  8.0 88.1 %collective-permute-start.2 = (bf16[512,512]{1,0:T(8,128)(2,1)}, bf16[512,512]{1,0:T(8,128)(2,1)S(1)}, u32[]{:S(2)}, u32[]{:S(2)}) collective-permute-start(bf16[512,512]{1,0:T(8,128)(2,1)} %param.19), channel_id=1, source_target_pairs={{0,4},{4,8},{8,12},{12,0},{1,5},{5,9},{9,13},{13,1},{2,6},{6,10},{... | collective-permute-start | bytes 1572872 | tf_op jit(solution)/shard_map/ppermute | solution.py:20
  11.1 153.6 %collective-permute-start.4 = (bf16[512,512]{1,0:T(8,128)(2,1)}, bf16[512,512]{1,0:T(8,128)(2,1)S(1)}, u32[]{:S(2)}, u32[]{:S(2)}) collective-permute-start(bf16[512,512]{1,0:T(8,128)(2,1)} %param.19), channel_id=1, source_target_pairs={{0,12},{4,0},{8,4},{12,8},{1,13},{5,1},{9,5},{13,9},{2,14},{6,2},{... | collective-permute-start | bytes 1572872 | tf_op jit(solution)/shard_map/ppermute | solution.py:22
  15.8 144.6 %collective-permute-start = (bf16[8,512]{1,0:T(8,128)(2,1)S(1)}, bf16[8,512]{1,0:T(8,128)(2,1)S(1)}, u32[]{:S(2)}, u32[]{:S(2)}) collective-permute-start(bf16[8,512]{1,0:T(8,128)(2,1)S(1)} %get-tuple-element.102), channel_id=1, source_target_pairs={{0,4},{4,8},{8,12},{1,5},{5,9},{9,13},{2,6},{6,10},{10,14},{3,7},{... | collective-permute-start | bytes 24584 | tf_op jit(solution)/shard_map/ppermute | solution.py:35
  17.6 142.7 %collective-permute-start.1 = (bf16[8,512]{1,0:T(8,128)(2,1)S(1)}, bf16[8,512]{1,0:T(8,128)(2,1)S(1)}, u32[]{:S(2)}, u32[]{:S(2)}) collective-permute-start(bf16[8,512]{1,0:T(8,128)(2,1)S(1)} %get-tuple-element.103), channel_id=1, source_target_pairs={{4,0},{8,4},{12,8},{5,1},{9,5},{13,9},{6,2},{10,6},{14,10},{7,3},{... | collective-permute-start | bytes 24584 | tf_op jit(solution)/shard_map/ppermute | solution.py:37
  19.0 144.8 %copy-start = (bf16[512,512]{1,0:T(8,128)(2,1)S(1)}, bf16[512,512]{1,0:T(8,128)(2,1)}, u32[]{:S(2)}) copy-start(bf16[512,512]{1,0:T(8,128)(2,1)} %param.19) | copy-start | bytes 1572868
  19.0 199.8 %reduce-scatter.2.cloned.1.call-start = ((), (), s32[]{:S(2)}) async-start(), calls=%async_computation.3 | async-start | bytes 819200 | tf_op jit(solution)/shard_map/reduce_scatter | solution.py:158
  96.0 66.0 %collective-permute-start.3 = (bf16[512,512]{1,0:T(8,128)(2,1)S(1)}, bf16[512,512]{1,0:T(8,128)(2,1)S(1)}, u32[]{:S(2)}, u32[]{:S(2)}) collective-permute-start(bf16[512,512]{1,0:T(8,128)(2,1)S(1)} %collective-permute-done.2), channel_id=1, source_target_pairs={{0,4},{4,8},{8,12},{12,0},{1,5},{5,9},{9,13},{13,1},{2,6},{6,10},{... | collective-permute-start | bytes 1572872 | tf_op jit(solution)/shard_map/ppermute | solution.py:20
  171.4 16.3 %copy-start.5 = (f32[4]{0:T(128)S(1)}, f32[4]{0:T(128)}, u32[]{:S(2)}) copy-start(f32[4]{0:T(128)} %param.16) | copy-start | bytes 52
  171.4 16.6 %copy-start.4 = (f32[4,128]{1,0:T(4,128)S(1)}, f32[4,128]{1,0:T(4,128)}, u32[]{:S(2)}) copy-start(f32[4,128]{1,0:T(4,128)} %param.17) | copy-start | bytes 6148
  187.4 3.0 %copy-start.1 = (bf16[160,512]{1,0:T(8,128)(2,1)S(1)}, bf16[160,512]{1,0:T(8,128)(2,1)}, u32[]{:S(2)}) copy-start(bf16[160,512]{1,0:T(8,128)(2,1)} %constant_dynamic-slice_fusion.1) | copy-start | bytes 491524
  187.4 3.0 %copy-start.2 = (bf16[176,512]{1,0:T(8,128)(2,1)S(1)}, bf16[176,512]{1,0:T(8,128)(2,1)}, u32[]{:S(2)}) copy-start(bf16[176,512]{1,0:T(8,128)(2,1)} %pad_maximum_fusion) | copy-start | bytes 540676
Sparse Core Ops, SparseCore 0:
  9.5 69.5 all-gather.2
  80.7 59.4 all-gather.4
  194.9 23.8 reduce-scatter.1
